TPU v7x, 32 devices: a whole 2x2x4 slice. The times are simulated.
32 devices in a mesh: sp: 16 (over z, y, x), tp: 2 (over core).
Axes of the slice: x: 2, y: 2, z: 4, core: 2. Of those that a mesh axis runs over, the one named last changes fastest.
Arguments:
- residual: bfloat16 [2048, 2048], P('sp'), may hold values from -6 to 6
- query_nope: bfloat16 [2048, 8, 128], P('sp', 'tp'), may hold values from -6 to 6
- query_rope: bfloat16 [2048, 8, 64], P('sp', 'tp'), may hold values from -64 to 64
- latent: bfloat16 [2048, 256], P('sp'), may hold values from -6 to 6
- rope_key: bfloat16 [2048, 64], P('sp'), may hold values from -64 to 64
- kv_gain: bfloat16 [256], replicated, may hold values from 0.099609375 to 1.8984375
- key_up: bfloat16 [256, 8, 128], replicated, may hold values from -0.375 to 0.375
- value_up: bfloat16 [256, 8, 128], replicated, may hold values from -0.375 to 0.375
- out_weight: bfloat16 [1024, 2048], P('tp'), may hold values from -0.1875 to 0.1875
- post_gain: bfloat16 [2048], replicated, may hold values from 0.099609375 to 1.8984375
- pre_gain: bfloat16 [2048], replicated, may hold values from 0.099609375 to 1.8984375
- ffn_gain: bfloat16 [2048], replicated, may hold values from 0.099609375 to 1.8984375
- up_value: bfloat16 [2048, 5632], P('sp', 'tp'), may hold values from -0.125 to 0.125
- up_gate: bfloat16 [2048, 5632], P('sp', 'tp'), may hold values from -0.125 to 0.125
- conv_value: bfloat16 [3, 5632], replicated, may hold values from -3.5 to 3.5
- conv_gate: bfloat16 [3, 5632], replicated, may hold values from -3.5 to 3.5
- down_weight: bfloat16 [5632, 2048], P('tp', 'sp'), may hold values from -0.078125 to 0.078125
Outputs:
- layer_out: bfloat16 [2048, 2048], P(('sp', 'tp'))
All inputs are finite; a program needn't handle non-finite values.
Results may differ from a plain program's by a relative error of at most 0.02.
Values may be sent and summed in bfloat16 or wider, within the bound.
No kernel may reach another device: no remote copies, remote signals or barrier semaphores. Data moves between devices by JAX's collectives and lax.ppermute only.
A program may use at most 128 MiB of HBM per device.

v0:
```python
import jax
import jax.numpy as jnp
from jax import lax
from jax.sharding import PartitionSpec as P

GRID = 64
epsilon = 1e-06
rope_base = 10000.0


def extended(x, sides, width):
    for axis, dim in sides:
        size, length = (lax.axis_size(axis), x.shape[dim])
        up = [(i, (i + 1) % size) for i in range(size - 1)]
        down = [(j, i) for i, j in up]
        last = lax.slice_in_dim(x, length - width, length, axis=dim)
        initial = lax.slice_in_dim(x, 0, width, axis=dim)
        before = lax.ppermute(last, axis, up)
        after = lax.ppermute(initial, axis, down)
        x = jnp.concatenate([before, x, after], axis=dim)
    return x


def rms_norm(values, gain):
    return (
        values
        * lax.rsqrt(jnp.mean(values * values, axis=-1, keepdims=True) + epsilon)
        * gain.astype(jnp.float32)
    )


def widened(values):
    return lax.optimization_barrier(values.astype(jnp.bfloat16)).astype(jnp.float32)


def rotate(values, positions):
    pair_count = values.shape[-1] // 4
    frequency = rope_base ** (-jnp.arange(pair_count, dtype=jnp.float32) / pair_count)
    grid_rows = (positions // GRID).astype(jnp.float32)
    grid_cols = (positions % GRID).astype(jnp.float32)
    angles = jnp.stack([grid_rows, grid_cols], axis=-1)[:, :, None] * frequency
    table_shape = (angles.shape[0],) + (1,) * (values.ndim - 2) + angles.shape[1:]
    cosine = jnp.cos(angles).reshape(table_shape)
    sine = jnp.sin(angles).reshape(table_shape)
    halves = values.reshape(values.shape[:-1] + (2, 2, pair_count))
    leading = halves[..., 0, :]
    trailing = halves[..., 1, :]
    turned = jnp.stack(
        [leading * cosine - trailing * sine, trailing * cosine + leading * sine], axis=-2
    )
    return turned.reshape(values.shape)


def body(
    residual,
    query_nope,
    query_rope,
    latent,
    rope_key,
    kv_gain,
    key_up,
    value_up,
    out_weight,
    post_gain,
    pre_gain,
    ffn_gain,
    up_value,
    up_gate,
    conv_value,
    conv_gate,
    down_weight,
):
    tok_rows = residual.shape[0]
    heads_dev = query_nope.shape[1]
    value_width = value_up.shape[2]
    tp_index = lax.axis_index("tp")
    positions = lax.axis_index("sp") * tok_rows + jnp.arange(tok_rows, dtype=jnp.int32)
    score_scale = (query_nope.shape[2] + query_rope.shape[2]) ** (-0.5)
    normed = rms_norm(latent.astype(jnp.float32), kv_gain).astype(jnp.bfloat16)
    key_turn = rotate(rope_key.astype(jnp.float32), positions).astype(jnp.bfloat16)
    query_turn = rotate(query_rope.astype(jnp.float32), positions).astype(jnp.bfloat16)
    key_local = lax.dynamic_slice_in_dim(key_up, tp_index * heads_dev, heads_dev, 1)
    value_local = lax.dynamic_slice_in_dim(value_up, tp_index * heads_dev, heads_dev, 1)
    pieces = (
        lax.all_gather(normed, "sp", axis=0, tiled=True),
        lax.all_gather(key_turn, "sp", axis=0, tiled=True),
    )
    keys_nope = jnp.einsum(
        "nc,chd->nhd", pieces[0], key_local, preferred_element_type=jnp.float32
    ).astype(jnp.bfloat16)
    values_part = jnp.einsum(
        "nc,chd->nhd", pieces[0], value_local, preferred_element_type=jnp.float32
    ).astype(jnp.bfloat16)
    row_max = jnp.full((heads_dev, tok_rows), -1e30, jnp.float32)
    scores = (
        jnp.einsum("qhd,khd->hqk", query_nope, keys_nope, preferred_element_type=jnp.float32)
        + jnp.einsum("qhd,kd->hqk", query_turn, pieces[1], preferred_element_type=jnp.float32)
    ) * score_scale
    new_max = jnp.maximum(row_max, jnp.max(scores, axis=-1))
    weights = jnp.exp(scores - new_max[:, :, None])
    totals = jnp.sum(weights, axis=-1)
    weighted = jnp.einsum(
        "hqk,khd->hqd",
        weights.astype(jnp.bfloat16),
        values_part,
        preferred_element_type=jnp.float32,
    )
    attended = (weighted / totals[:, :, None]).astype(jnp.bfloat16)
    attended = jnp.transpose(attended, (1, 0, 2)).reshape(tok_rows, heads_dev * value_width)
    row_share = tok_rows // lax.axis_size("tp")
    summed = lax.psum_scatter(
        jnp.dot(attended, out_weight, preferred_element_type=jnp.float32).astype(jnp.bfloat16),
        "tp",
        scatter_dimension=0,
        tiled=True,
    ).astype(jnp.float32)
    own_rows = lax.dynamic_slice_in_dim(residual, tp_index * row_share, row_share, 0).astype(
        jnp.float32
    )
    stream_wide = widened(own_rows + rms_norm(widened(summed), post_gain))
    inputs = lax.all_gather(
        rms_norm(stream_wide, pre_gain).astype(jnp.bfloat16), "tp", axis=0, tiled=True
    )
    ff_dev = up_value.shape[1]
    up_joined = jnp.concatenate([up_value, up_gate], axis=1)
    up_whole = lax.all_gather(up_joined, "sp", axis=0, tiled=True)
    up_pair = jnp.dot(inputs, up_whole, preferred_element_type=jnp.float32).astype(jnp.bfloat16)
    padded = extended(up_pair, (("sp", 0),), 1).astype(jnp.float32)
    channel_start = tp_index * ff_dev
    conv_taps = jnp.concatenate(
        [
            lax.dynamic_slice_in_dim(conv_value, channel_start, ff_dev, 1),
            lax.dynamic_slice_in_dim(conv_gate, channel_start, ff_dev, 1),
        ],
        axis=1,
    ).astype(jnp.float32)
    mixed_conv = (
        padded[:-2] * conv_taps[0] + padded[1:-1] * conv_taps[1] + padded[2:] * conv_taps[2]
    )
    hidden = (jax.nn.silu(mixed_conv[:, ff_dev:]) * mixed_conv[:, :ff_dev]).astype(jnp.bfloat16)
    down_whole = lax.all_gather(down_weight, "sp", axis=1, tiled=True)
    down_terms = jnp.dot(hidden, down_whole, preferred_element_type=jnp.float32)
    reduced = lax.psum_scatter(
        down_terms.astype(jnp.bfloat16), "tp", scatter_dimension=0, tiled=True
    ).astype(jnp.float32)
    return (stream_wide + rms_norm(widened(reduced), ffn_gain)).astype(jnp.bfloat16)


def solution(mesh):
    placed = (
        P("sp", None),
        P("sp", "tp", None),
        P("sp", "tp", None),
        P("sp", None),
        P("sp", None),
        P(),
        P(),
        P(),
        P("tp", None),
        P(),
        P(),
        P(),
        P("sp", "tp"),
        P("sp", "tp"),
        P(),
        P(),
        P("tp", "sp"),
    )
    return jax.shard_map(
        body, mesh=mesh, in_specs=placed, out_specs=P(("sp", "tp"), None), check_vma=False
    )
```

profile of v0, /device:TPU:0, one launch (start us, length us, event | category | flops | bytes accessed | tf_op | source)
XLA Modules:
  0.0 553.0 jit_solution(2200279591683789855)
XLA Ops:
  8.3 1.6 fusion.42
  11.9 44.1 %all_gather.16 = bf16[2048,64]{0,1:T(8,128)(2,1)S(1)} all-gather(bf16[128,64]{0,1:T(8,128)(2,1)S(1)} %bitcast.41), channel_id=1, replica_groups=mesh['sp'=16,'tp'=2] {'sp'}, dimensions={0}, use_global_device_ids=true | all-gather | bytes 278528 | tf_op jit(solution)/shard_map/all_gather | solution.py:86
  56.0 1.5 constant_dynamic-slice_fusion.2
  57.5 10.8 %all-gather.4.cloned.1.call-done = bf16[2048,256]{1,0:T(8,128)(2,1)} async-done(((bf16[128,256]{1,0:T(8,128)(2,1)}), bf16[2048,256]{1,0:T(8,128)(2,1)}) %all-gather.4.cloned.1.call-update) | async-done | bytes 1048592 | tf_op jit(solution)/shard_map/all_gather | solution.py:85
  68.3 4.4 fusion.8
  72.7 2.9 fusion.58
  75.7 1.9 copy-done.1
  78.2 4.3 fusion.16
  82.5 2.3 convolution_convert_fusion.4
  84.8 1.2 pad_maximum_fusion
  87.5 4.2 reduce-scatter.3.cloned.1.call-done
  92.8 1.2 fusion.28
  94.3 2.2 all_gather.17
  96.5 249.5 %all-gather.6.cloned.1.call-done = bf16[2048,5632]{1,0:T(8,128)(2,1)} async-done(((bf16[128,5632]{1,0:T(8,128)(2,1)}), bf16[2048,5632]{1,0:T(8,128)(2,1)}) %all-gather.6.cloned.1.call-update) | async-done | bytes 23068688 | tf_op jit(solution)/shard_map/all_gather | solution.py:126
  346.1 10.7 %convolution_convert_fusion = bf16[128,5632]{1,0:T(8,128)(2,1)S(1)} fusion(bf16[128,2048]{1,0:T(8,128)(2,1)S(1)} %all_gather.17, bf16[2048,5632]{1,0:T(8,128)(2,1)} %all-gather.6.cloned.1.call-done), kind=kOutput, calls=%fused_computation | convolution fusion | flops 2953510912 | bytes 25034752 | tf_op jit(solution)/shard_map/dot_general | solution.py:127
  356.8 3.4 collective-permute-start
  360.2 1.5 collective-permute-start.1
  362.1 4.4 collective-permute-done.1
  366.9 2.4 fusion.3
  369.4 160.2 %all-gather.8.cloned.1.call-done = bf16[2816,2048]{1,0:T(8,128)(2,1)} async-done(((bf16[2816,128]{1,0:T(8,128)(2,1)}), bf16[2816,2048]{1,0:T(8,128)(2,1)}) %all-gather.8.cloned.1.call-update) | async-done | bytes 11534352 | tf_op jit(solution)/shard_map/all_gather | solution.py:141
  529.5 7.7 %convolution_convert_fusion.3 = bf16[128,2048]{1,0:T(8,128)(2,1)} fusion(bf16[2816,2048]{1,0:T(8,128)(2,1)} %all-gather.8.cloned.1.call-done, f32[128,5632]{1,0:T(8,128)} %fusion.3), kind=kOutput, calls=%fused_computation.13 | convolution fusion | flops 1478819840 | bytes 14942208 | tf_op jit(solution)/shard_map/dot_general | solution.py:142
  537.3 6.2 %reduce-scatter.5.cloned.1.call-done = bf16[64,2048]{1,0:T(8,128)(2,1)} async-done(((bf16[128,2048]{1,0:T(8,128)(2,1)}), bf16[64,2048]{1,0:T(8,128)(2,1)}) %reduce-scatter.5.cloned.1.call-update) | async-done | bytes 262160 | tf_op jit(solution)/shard_map/reduce_scatter | solution.py:143
  543.5 1.1 fusion.29
  544.6 1.8 fusion.34
  (54 shorter events, 8.1 us)
Async XLA Ops:
  6.5 75.9 %copy-start = (bf16[512,2048]{1,0:T(8,128)(2,1)S(1)}, bf16[512,2048]{1,0:T(8,128)(2,1)}, u32[]{:S(2)}) copy-start(bf16[512,2048]{1,0:T(8,128)(2,1)} %param.25) | copy-start | bytes 6291460
  6.5 61.8 %all-gather.4.cloned.1.call-start = ((), (), s32[]{:S(2)}) async-start(), calls=%async_computation.2 | async-start | bytes 1114112 | tf_op jit(solution)/shard_map/all_gather | solution.py:85
  9.9 81.8 %reduce-scatter.3.cloned.1.call-start = ((), (), s32[]{:S(2)}) async-start(), calls=%async_computation.3 | async-start | bytes 786432 | tf_op jit(solution)/shard_map/reduce_scatter | solution.py:111
  75.7 1.9 copy-start.1
  75.7 2.5 copy-start.2
  82.5 2.4 copy-start.3
  82.5 2.4 copy-start.4
  84.7 2.0 copy-start.5
  84.8 2.0 copy-start.6
  84.8 261.3 %all-gather.6.cloned.1.call-start = ((), (), s32[]{:S(2)}) async-start(), calls=%async_computation.4 | async-start | bytes 24510464 | tf_op jit(solution)/shard_map/all_gather | solution.py:126
  86.1 443.5 %all-gather.8.cloned.1.call-start = ((), (), s32[]{:S(2)}) async-start(), calls=%async_computation.5 | async-start | bytes 12255232 | tf_op jit(solution)/shard_map/all_gather | solution.py:141
  86.7 456.9 %reduce-scatter.5.cloned.1.call-start = ((), (), s32[]{:S(2)}) async-start(), calls=%async_computation.6 | async-start | bytes 786432 | tf_op jit(solution)/shard_map/reduce_scatter | solution.py:143
  356.8 5.3 collective-permute-start
  360.2 6.3 %collective-permute-start.1 = (bf16[1,5632]{1,0:T(2,128)(2,1)S(1)}, bf16[1,5632]{1,0:T(2,128)(2,1)S(1)}, u32[]{:S(2)}, u32[]{:S(2)}) collective-permute-start(bf16[1,5632]{1,0:T(2,128)(2,1)S(1)} %get-tuple-element.9), channel_id=1, source_target_pairs={{2,0},{4,2},{6,4},{8,6},{10,8},{12,10},{14,12},{16,14},{18,16},{20... | collective-permute-start | bytes 33800 | tf_op jit(solution)/shard_map/ppermute | solution.py:19
  369.4 167.9 %copy-start.7 = (bf16[2048]{0:T(1024)(128)(2,1)S(1)}, bf16[2048]{0:T(1024)(128)(2,1)}, u32[]{:S(2)}) copy-start(bf16[2048]{0:T(1024)(128)(2,1)} %param.28) | copy-start | bytes 12292
Sparse Core Ops, SparseCore 0:
  10.1 58.1 all-gather.3
  84.9 6.7 reduce-scatter.2
  94.4 251.6 all-gather.5
  348.6 180.8 all-gather.7
  537.4 6.0 reduce-scatter.4
where the time goes:
time: 554 us; the launch traced here: 553 us
  waiting for transfers between devices  436 us (79%)
  blocking collectives  46.3 us (8%)
  matrix products  32.3 us (6%)
  other arithmetic  15.6 us (3%)
  between operations  13.4 us (2%)
    all_gather x1, waiting for transfers between devices, body(): up_whole = lax.all_gather(up_joined, 'sp', axis=0, tiled=True)  250 us
    all_gather x1, waiting for transfers between devices, body(): down_whole = lax.all_gather(down_weight, 'sp', axis=1, tiled=True)  160 us
    all_gather x1, blocking collectives, body(): lax.all_gather(key_turn, 'sp', axis=0, tiled=True)  44.1 us
  transfers between devices with their start and end apart: 7, of which 7 were waited for; matrix products, arithmetic and copies ran while one was open for 4% of the time, Pallas kernels for 0%

commit v1 on v0

--- a/solution.py
+++ b/solution.py
@@ -138,7 +138,7 @@
         padded[:-2] * conv_taps[0] + padded[1:-1] * conv_taps[1] + padded[2:] * conv_taps[2]
     )
     hidden = (jax.nn.silu(mixed_conv[:, ff_dev:]) * mixed_conv[:, :ff_dev]).astype(jnp.bfloat16)
-    down_whole = lax.all_gather(down_weight, "sp", axis=1, tiled=True)
+    down_whole = jnp.concatenate(lax.all_gather(down_weight, "sp"), axis=1)
     down_terms = jnp.dot(hidden, down_whole, preferred_element_type=jnp.float32)
     reduced = lax.psum_scatter(
         down_terms.astype(jnp.bfloat16), "tp", scatter_dimension=0, tiled=True

time: 554 us -> 533 us (0.962)
  waiting for transfers between devices: 436 us -> 399 us
  local copies, waits for them, and re-layouts: 4.22 us -> 21.4 us
    all_gather x1, waiting for transfers between devices: 160 us -> 127 us  [body(): down_whole = jnp.concatenate(lax.all_gather(down_weight, 'sp'), axis=1)]
    reshape x0 -> x1, local copies, waits for them, and re-layouts: none -> 15.1 us  [body(): down_whole = jnp.concatenate(lax.all_gather(down_weight, 'sp'), axis=1)]
  transfers between devices with their start and end apart: 7 -> 7, of which waited for: 7 -> 5; matrix products, arithmetic and copies ran while one was open for 4% -> 6% of each run, Pallas kernels for 0% -> 0%
where the time goes in v1:
time: 533 us; the launch traced here: 532 us
  waiting for transfers between devices  399 us (75%)
  blocking collectives  46.3 us (9%)
  matrix products  31.4 us (6%)
  local copies, waits for them, and re-layouts  21.4 us (4%)
  other arithmetic  15.6 us (3%)
  between operations  13.4 us (3%)
    all_gather x1, waiting for transfers between devices, body(): up_whole = lax.all_gather(up_joined, 'sp', axis=0, tiled=True)  250 us
    all_gather x1, waiting for transfers between devices, body(): down_whole = jnp.concatenate(lax.all_gather(down_weight, 'sp'), axis=1)  127 us
    all_gather x1, blocking collectives, body(): lax.all_gather(key_turn, 'sp', axis=0, tiled=True)  44.1 us
    reshape x1, local copies, waits for them, and re-layouts, body(): down_whole = jnp.concatenate(lax.all_gather(down_weight, 'sp'), axis=1)  15.1 us
    all_gather x1, waiting for transfers between devices, body(): lax.all_gather(normed, 'sp', axis=0, tiled=True)  10.8 us
    dot_general x1, matrix products, body(): jnp.dot(inputs, up_whole, preferred_element_type=jnp.float32)  10.7 us
  transfers between devices with their start and end apart: 7, of which 5 were waited for; matrix products, arithmetic and copies ran while one was open for 6% of the time, Pallas kernels for 0%

profile of v1, /device:TPU:0, one launch (start us, length us, event | category | flops | bytes accessed | tf_op | source)
XLA Modules:
  0.0 532.2 jit_solution(3721203452813544153)
XLA Ops:
  8.3 1.6 fusion.42
  11.9 44.1 %all_gather.19 = bf16[2048,64]{0,1:T(8,128)(2,1)S(1)} all-gather(bf16[128,64]{0,1:T(8,128)(2,1)S(1)} %bitcast.47), channel_id=1, replica_groups=mesh['sp'=16,'tp'=2] {'sp'}, dimensions={0}, use_global_device_ids=true | all-gather | bytes 278528 | tf_op jit(solution)/shard_map/all_gather | solution.py:86
  56.0 1.5 constant_dynamic-slice_fusion.2
  57.5 10.8 %all-gather.5.cloned.1.call-done = bf16[2048,256]{1,0:T(8,128)(2,1)} async-done(((bf16[128,256]{1,0:T(8,128)(2,1)}), bf16[2048,256]{1,0:T(8,128)(2,1)}) %all-gather.5.cloned.1.call-update) | async-done | bytes 1048592 | tf_op jit(solution)/shard_map/all_gather | solution.py:85
  68.3 4.4 fusion.8
  72.7 2.9 fusion.58
  75.7 1.9 copy-done.2
  78.2 4.4 fusion.16
  82.7 2.3 convolution_convert_fusion.4
  85.1 1.2 pad_maximum_fusion
  87.0 4.9 reduce-scatter.3.cloned.1.call-done
  93.0 1.1 fusion.28
  94.5 2.2 all_gather.20
  96.7 249.6 %all-gather.7.cloned.1.call-done = bf16[2048,5632]{1,0:T(8,128)(2,1)} async-done(((bf16[128,5632]{1,0:T(8,128)(2,1)}), bf16[2048,5632]{1,0:T(8,128)(2,1)}) %all-gather.7.cloned.1.call-update) | async-done | bytes 23068688 | tf_op jit(solution)/shard_map/all_gather | solution.py:126
  346.3 10.7 %convolution_convert_fusion = bf16[128,5632]{1,0:T(8,128)(2,1)S(1)} fusion(bf16[128,2048]{1,0:T(8,128)(2,1)S(1)} %all_gather.20, bf16[2048,5632]{1,0:T(8,128)(2,1)} %all-gather.7.cloned.1.call-done), kind=kOutput, calls=%fused_computation | convolution fusion | flops 2953510912 | bytes 25034752 | tf_op jit(solution)/shard_map/dot_general | solution.py:127
  357.1 3.4 collective-permute-start
  360.4 1.5 collective-permute-start.1
  362.1 126.9 %all-gather.9.cloned.1.call-done = bf16[45056,128]{1,0:T(8,128)(2,1)} async-done(((bf16[2816,128]{1,0:T(8,128)(2,1)}), bf16[45056,128]{1,0:T(8,128)(2,1)}) %all-gather.9.cloned.1.call-update) | async-done | bytes 11534352 | tf_op jit(solution)/shard_map/all_gather | solution.py:141
  489.0 15.1 %copy.27 = bf16[2816,16,128]{0,2,1:T(8,128)(2,1)} copy(bf16[2816,16,128]{2,0,1:T(8,128)(2,1)} %bitcast.42) | data formatting | bytes 23068672 | tf_op jit(solution)/shard_map/reshape | solution.py:141
  504.6 2.5 fusion.3
  507.1 2.8 copy-done.3
  509.9 6.6 %convolution_convert_fusion.3 = bf16[128,2048]{1,0:T(8,128)(2,1)} fusion(bf16[2816,2048]{0,1:T(8,128)(2,1)S(1)} %bitcast.43, f32[128,5632]{1,0:T(8,128)} %fusion.3), kind=kOutput, calls=%fused_computation.13 | convolution fusion | flops 1478819840 | bytes 14942208 | tf_op jit(solution)/shard_map/dot_general | solution.py:142
  516.5 6.2 %reduce-scatter.5.cloned.1.call-done = bf16[64,2048]{1,0:T(8,128)(2,1)} async-done(((bf16[128,2048]{1,0:T(8,128)(2,1)}), bf16[64,2048]{1,0:T(8,128)(2,1)}) %reduce-scatter.5.cloned.1.call-update) | async-done | bytes 262160 | tf_op jit(solution)/shard_map/reduce_scatter | solution.py:143
  523.9 1.8 fusion.34
  (65 shorter events, 8.3 us)
Async XLA Ops:
  6.5 76.1 %copy-start = (bf16[512,2048]{1,0:T(8,128)(2,1)S(1)}, bf16[512,2048]{1,0:T(8,128)(2,1)}, u32[]{:S(2)}) copy-start(bf16[512,2048]{1,0:T(8,128)(2,1)} %param.25) | copy-start | bytes 6291460
  6.5 61.8 %all-gather.5.cloned.1.call-start = ((), (), s32[]{:S(2)}) async-start(), calls=%async_computation.2 | async-start | bytes 1114112 | tf_op jit(solution)/shard_map/all_gather | solution.py:85
  9.9 82.0 %reduce-scatter.3.cloned.1.call-start = ((), (), s32[]{:S(2)}) async-start(), calls=%async_computation.3 | async-start | bytes 786432 | tf_op jit(solution)/shard_map/reduce_scatter | solution.py:111
  75.7 1.9 copy-start.2
  75.7 2.5 copy-start.4
  82.6 2.4 copy-start.5
  82.6 2.4 copy-start.6
  84.9 2.0 copy-start.10
  84.9 2.0 copy-start.11
  84.9 2.0 copy-start.8
  84.9 2.0 copy-start.9
  85.0 8.1 %copy-start.7 = (bf16[128,2048]{1,0:T(8,128)(2,1)S(1)}, bf16[128,2048]{1,0:T(8,128)(2,1)}, u32[]{:S(2)}) copy-start(bf16[128,2048]{1,0:T(8,128)(2,1)} %param.17) | copy-start | bytes 1572868
  85.0 261.3 %all-gather.7.cloned.1.call-start = ((), (), s32[]{:S(2)}) async-start(), calls=%async_computation.4 | async-start | bytes 24510464 | tf_op jit(solution)/shard_map/all_gather | solution.py:126
  86.3 402.7 %all-gather.9.cloned.1.call-start = ((), (), s32[]{:S(2)}) async-start(), calls=%async_computation.6 | async-start | bytes 12255232 | tf_op jit(solution)/shard_map/all_gather | solution.py:141
  86.8 435.9 %reduce-scatter.5.cloned.1.call-start = ((), (), s32[]{:S(2)}) async-start(), calls=%async_computation.5 | async-start | bytes 786432 | tf_op jit(solution)/shard_map/reduce_scatter | solution.py:143
  357.1 147.0 %collective-permute-start = (bf16[1,5632]{1,0:T(2,128)(2,1)S(1)}, bf16[1,5632]{1,0:T(2,128)(2,1)S(1)}, u32[]{:S(2)}, u32[]{:S(2)}) collective-permute-start(bf16[1,5632]{1,0:T(2,128)(2,1)S(1)} %get-tuple-element.8), channel_id=1, source_target_pairs={{0,2},{2,4},{4,6},{6,8},{8,10},{10,12},{12,14},{14,16},{16,18},{18... | collective-permute-start | bytes 33800 | tf_op jit(solution)/shard_map/ppermute | solution.py:18
  360.4 143.7 %collective-permute-start.1 = (bf16[1,5632]{1,0:T(2,128)(2,1)S(1)}, bf16[1,5632]{1,0:T(2,128)(2,1)S(1)}, u32[]{:S(2)}, u32[]{:S(2)}) collective-permute-start(bf16[1,5632]{1,0:T(2,128)(2,1)S(1)} %get-tuple-element.9), channel_id=1, source_target_pairs={{2,0},{4,2},{6,4},{8,6},{10,8},{12,10},{14,12},{16,14},{18,16},{20... | collective-permute-start | bytes 33800 | tf_op jit(solution)/shard_map/ppermute | solution.py:19
  504.5 5.3 copy-start.3
  509.9 6.6 %copy-start.12 = (bf16[2048]{0:T(1024)(128)(2,1)S(1)}, bf16[2048]{0:T(1024)(128)(2,1)}, u32[]{:S(2)}) copy-start(bf16[2048]{0:T(1024)(128)(2,1)} %param.28) | copy-start | bytes 12292
  509.9 15.8 %copy-start.1 = (bf16[512,2048]{1,0:T(8,128)(2,1)S(1)}, bf16[512,2048]{1,0:T(8,128)(2,1)}, u32[]{:S(2)}) copy-start(bf16[512,2048]{1,0:T(8,128)(2,1)} %param.25) | copy-start | bytes 6291460
Sparse Core Ops, SparseCore 0:
  10.1 58.1 all-gather.4
  85.1 6.7 reduce-scatter.2
  94.6 251.6 all-gather.6
  348.9 140.0 all-gather.8
  516.6 6.0 reduce-scatter.4
